TPU v7x, 32 devices: a whole 2x2x4 slice. The times are simulated.
32 devices in a mesh: sp: 8 (over z, x), tp: 4 (over y, core).
Axes of the slice: x: 2, y: 2, z: 4, core: 2. Of those that a mesh axis runs over, the one named last changes fastest.
Arguments:
- resid: bfloat16 [4096, 2048], P(('sp', 'tp')), may hold values from -6 to 6
- recurrent_input: bfloat16 [4096, 2048], P('sp', 'tp'), may hold values from -12.2 to 12.2
- recurrent_out_gate: bfloat16 [4096, 2048], P('sp', 'tp'), may hold values from -6 to 6
- filter_weight: float32 [4, 2048], P(None, 'tp'), may hold values from -3 to 3
- recurrence_gate_matrix: bfloat16 [32, 64, 64], P('tp'), may hold values from -0.75 to 0.75
- input_gate_matrix: bfloat16 [32, 64, 64], P('tp'), may hold values from -0.75 to 0.75
- channel_decay_raw: float32 [2048], P('tp'), may hold values from 4.8 to 13.5
- token_decay_boost: float32 [4096, 2048], P('sp', 'tp'), may hold values from -0.7 to 0
- output_projection_weight: bfloat16 [2048, 2048], P('tp'), may hold values from -0.375 to 0.375
- expert_norm_gain: float32 [2048], replicated, may hold values from 0.1 to 1.9
- routes: int32 [4096, 2], P('sp'), may hold values from 0 to 7, all different within a row; in each aligned block of 128 rows (0 to 127, 128 to 255, ...) at most 48 rows name the same one
- expert_pair_weight: float32 [4096, 2], P(('sp', 'tp')), may hold values from 0.2 to 0.8
- gate_weight: bfloat16 [8, 2048, 2048], P('sp', None, 'tp'), may hold values from -0.125 to 0.125
- up_weight: bfloat16 [8, 2048, 2048], P('sp', None, 'tp'), may hold values from -0.125 to 0.125
- down_weight: bfloat16 [8, 2048, 2048], P('sp', None, 'tp'), may hold values from -0.25 to 0.25
Outputs:
- layer_out: bfloat16 [4096, 2048], P(('sp', 'tp'))
Inputs may be any that keep to these rules, and one draw needn't show every extreme that they name: `routes`: in each aligned block of 128 rows no expert is named by more than 48 rows, and the two experts of a row differ.
All inputs are finite; a program needn't handle non-finite values.
Results may differ from a plain program's by a relative error of at most 0.013.
Values may be sent and summed in bfloat16 or wider, within the bound.
No kernel may reach another device: no remote copies, remote signals or barrier semaphores. Data moves between devices by JAX's collectives and lax.ppermute only.
A program may use at most 128 MiB of HBM per device.

v0:
```python
import jax
import jax.numpy as jnp
from jax import lax
from jax.sharding import PartitionSpec as P

RECURRENT_SCALE = 8.0
EPSILON = 1e-06


def shifted(block, axis, distance):
    devices = range(lax.axis_size(axis))
    route = [(i - distance, i) for i in devices if i - distance in devices]
    return lax.ppermute(block, axis, route)


def entering(x, axis, combine, identity):
    size, position = (lax.axis_size(axis), lax.axis_index(axis))
    everything = jax.tree.map(lambda part: lax.all_gather(part, axis), x)
    start = jax.tree.map(
        lambda part, zero: jnp.broadcast_to(jnp.asarray(zero, part.dtype), part.shape), x, identity
    )

    def lap(k, before):
        reached = k < position
        new = combine(before, jax.tree.map(lambda part: part[k], everything))
        return jax.tree.map(lambda a, b: jnp.where(reached, a, b), new, before)

    return lax.fori_loop(0, size, lap, start)


def chain_step(earlier, later):
    return (earlier[0] * later[0], later[0] * earlier[1] + later[1])


def slot_numbers(picks, experts):
    flat = picks.reshape(-1)
    onehot = (flat[:, None] == jnp.arange(experts, dtype=jnp.int32)[None, :]).astype(jnp.int32)
    before = jnp.cumsum(onehot, axis=0) - onehot
    return (flat, jnp.sum(before * onehot, axis=1))


def fill_slots(source_rows, slot_of, row_of, slot_count):
    match = slot_of[None, :] == jnp.arange(slot_count, dtype=jnp.int32)[:, None]
    picked = jnp.sum(jnp.where(match, row_of[None, :], 0), axis=1)
    present = jnp.any(match, axis=1)
    return jnp.where(present[:, None], source_rows[picked], jnp.zeros((), source_rows.dtype))


def expert_hidden(rows, gate_weight, up_weight):
    gate = jnp.dot(rows, gate_weight[0], preferred_element_type=jnp.float32)
    upward = jnp.dot(rows, up_weight[0], preferred_element_type=jnp.float32)
    return (jax.nn.silu(gate) * upward).astype(jnp.bfloat16)


def expert_down(active, down_weight):
    columns = down_weight[0]
    return jnp.dot(
        lax.all_gather(active, "tp", axis=1, tiled=True),
        columns,
        preferred_element_type=jnp.float32,
    ).astype(jnp.bfloat16)


def body(
    resid,
    recurrent_input,
    recurrent_out_gate,
    filter_weight,
    recurrence_gate_matrix,
    input_gate_matrix,
    channel_decay_raw,
    token_decay_boost,
    output_projection_weight,
    expert_norm_gain,
    routes,
    expert_pair_weight,
    gate_weight,
    up_weight,
    down_weight,
):
    tokens_here, channels = recurrent_input.shape
    taps = filter_weight.shape[0]
    rim = shifted(recurrent_input[tokens_here - taps + 1 :], "sp", 1)
    extended = jnp.concatenate([rim, recurrent_input], axis=0).astype(jnp.float32)
    mixed_in = extended[0:tokens_here] * filter_weight[0]
    for offset in range(1, taps):
        mixed_in = mixed_in + extended[offset : offset + tokens_here] * filter_weight[offset]
    smoothed = mixed_in.astype(jnp.bfloat16)
    grouped = smoothed.reshape(
        tokens_here, recurrence_gate_matrix.shape[0], recurrence_gate_matrix.shape[1]
    )
    recurrence_gate = jax.nn.sigmoid(
        jnp.einsum(
            "tni,nij->tnj", grouped, recurrence_gate_matrix, preferred_element_type=jnp.float32
        ).reshape(tokens_here, channels)
    )
    input_gate = jax.nn.sigmoid(
        jnp.einsum(
            "tni,nij->tnj", grouped, input_gate_matrix, preferred_element_type=jnp.float32
        ).reshape(tokens_here, channels)
    )
    decay_logarithm = (
        -RECURRENT_SCALE * recurrence_gate * jax.nn.softplus(-channel_decay_raw) + token_decay_boost
    )
    decay = jnp.exp(decay_logarithm)
    drive = jnp.sqrt(-jnp.expm1(2.0 * decay_logarithm)) * (
        input_gate * smoothed.astype(jnp.float32)
    )
    running, local_state = lax.associative_scan(chain_step, (decay, drive), axis=0)
    identity = (jnp.ones((channels,), jnp.float32), jnp.zeros((channels,), jnp.float32))
    carried = entering((running[-1], local_state[-1]), "sp", chain_step, identity)
    state = local_state + running * carried[1][None, :]
    branch = (jax.nn.gelu(recurrent_out_gate.astype(jnp.float32)) * state).astype(jnp.bfloat16)
    tp_size = lax.axis_size("tp")
    rows_dev = tokens_here // tp_size
    projected = lax.psum_scatter(
        jnp.dot(branch, output_projection_weight, preferred_element_type=jnp.float32),
        "tp",
        scatter_dimension=0,
        tiled=True,
    )
    stream = (resid.astype(jnp.float32) + projected).astype(jnp.bfloat16)
    stream_wide = stream.astype(jnp.float32)
    normed = (
        stream_wide
        * lax.rsqrt(jnp.mean(stream_wide * stream_wide, axis=1, keepdims=True) + EPSILON)
        * expert_norm_gain
    ).astype(jnp.bfloat16)
    model_width = normed.shape[1]
    experts = lax.axis_size("sp")
    capacity = max(2, 3 * rows_dev // experts)
    own_routes = lax.dynamic_slice_in_dim(routes, lax.axis_index("tp") * rows_dev, rows_dev, 0)
    own_flat, own_rank = slot_numbers(own_routes, experts)
    own_slots = own_flat * capacity + own_rank
    row_of = jnp.arange(2 * rows_dev, dtype=jnp.int32) // 2
    outgoing = fill_slots(normed, own_slots, row_of, experts * capacity).reshape(
        experts, capacity, model_width
    )
    arrived = lax.all_to_all(outgoing, "sp", split_axis=0, concat_axis=0, tiled=True)
    piece = lax.all_gather(
        arrived.reshape(1, experts * capacity, model_width), "tp", axis=0, tiled=True
    )
    flat_rows = piece.reshape(piece.shape[0] * piece.shape[1], model_width)
    active = expert_hidden(flat_rows, gate_weight, up_weight).reshape(
        piece.shape[0], piece.shape[1], -1
    )
    result = expert_down(active.reshape(-1, active.shape[2]), down_weight)
    joined = lax.all_to_all(
        result.reshape(tp_size, experts * capacity, -1),
        "tp",
        split_axis=0,
        concat_axis=2,
        tiled=True,
    )
    returned = lax.all_to_all(
        joined.reshape(experts, capacity, model_width),
        "sp",
        split_axis=0,
        concat_axis=0,
        tiled=True,
    )
    picked = (
        returned.reshape(experts * capacity, model_width)[own_slots]
        .astype(jnp.float32)
        .reshape(rows_dev, 2, model_width)
    )
    blended = jnp.sum(picked * expert_pair_weight[:, :, None], axis=1)
    return (stream_wide + blended).astype(jnp.bfloat16)


def solution(mesh):
    placed = (
        P(("sp", "tp"), None),
        P("sp", "tp"),
        P("sp", "tp"),
        P(None, "tp"),
        P("tp", None, None),
        P("tp", None, None),
        P("tp"),
        P("sp", "tp"),
        P("tp", None),
        P(),
        P("sp", None),
        P(("sp", "tp"), None),
        P("sp", None, "tp"),
        P("sp", None, "tp"),
        P("sp", None, "tp"),
    )
    return jax.shard_map(
        body, mesh=mesh, in_specs=placed, out_specs=P(("sp", "tp"), None), check_vma=False
    )
```

profile of v0, /device:TPU:0, one launch (start us, length us, event | category | flops | bytes accessed | tf_op | source)
XLA Modules:
  0.0 968.7 jit_solution(11987027139488644780)
XLA Ops:
  25.7 20.6 %slice.311 = f32[256,512]{0,1:T(8,128)} slice(f32[512,512]{0,1:T(8,128)} %get-tuple-element.134), slice={[0:511:2], [0:512:1]} | slice | bytes 1048576 | tf_op jit(solution)/shard_map/slice | solution.py:109
  46.4 20.7 %slice.312 = f32[256,512]{0,1:T(8,128)} slice(f32[512,512]{0,1:T(8,128)} %get-tuple-element.134), slice={[1:512:2], [0:512:1]} | slice | bytes 1048576 | tf_op jit(solution)/shard_map/slice | solution.py:109
  67.0 19.9 %slice.310 = f32[256,512]{0,1:T(8,128)} slice(f32[512,512]{0,1:T(8,128)S(1)} %get-tuple-element.135), slice={[1:512:2], [0:512:1]} | slice | bytes 1048576 | tf_op jit(solution)/shard_map/slice | solution.py:109
  87.0 19.9 %slice.314 = f32[256,512]{0,1:T(8,128)} slice(f32[512,512]{0,1:T(8,128)S(1)} %get-tuple-element.135), slice={[0:511:2], [0:512:1]} | slice | bytes 1048576 | tf_op jit(solution)/shard_map/slice | solution.py:109
  109.5 13.2 %slice.317 = f32[128,512]{0,1:T(8,128)} slice(f32[256,512]{0,1:T(8,128)} %get-tuple-element.138), slice={[0:255:2], [0:512:1]} | slice | bytes 524288 | tf_op jit(solution)/shard_map/slice | solution.py:109
  122.7 13.0 %slice.318 = f32[128,512]{0,1:T(8,128)} slice(f32[256,512]{0,1:T(8,128)} %get-tuple-element.138), slice={[1:256:2], [0:512:1]} | slice | bytes 524288 | tf_op jit(solution)/shard_map/slice | solution.py:109
  135.7 13.0 %slice.316 = f32[128,512]{0,1:T(8,128)} slice(f32[256,512]{0,1:T(8,128)} %get-tuple-element.139), slice={[1:256:2], [0:512:1]} | slice | bytes 524288 | tf_op jit(solution)/shard_map/slice | solution.py:109
  148.7 13.0 %slice.320 = f32[128,512]{0,1:T(8,128)} slice(f32[256,512]{0,1:T(8,128)} %get-tuple-element.139), slice={[0:255:2], [0:512:1]} | slice | bytes 524288 | tf_op jit(solution)/shard_map/slice | solution.py:109
  170.3 6.9 slice.324
  177.2 7.4 slice.322
  184.6 7.3 slice.326
  296.4 7.3 slice.321
  310.5 12.9 %slice.315 = f32[127,512]{0,1:T(8,128)} slice(f32[256,512]{0,1:T(8,128)} %get-tuple-element.139), slice={[2:256:2], [0:512:1]} | slice | bytes 520192 | tf_op jit(solution)/shard_map/slice | solution.py:109
  323.4 13.1 %slice.372 = f32[127,512]{0,1:T(8,128)} slice(f32[256,512]{0,1:T(8,128)} %get-tuple-element.138), slice={[2:256:2], [0:512:1]} | slice | bytes 520192 | tf_op jit(solution)/shard_map/slice | solution.py:109
  339.8 19.9 %slice.309 = f32[255,512]{0,1:T(8,128)} slice(f32[512,512]{0,1:T(8,128)S(1)} %get-tuple-element.135), slice={[2:512:2], [0:512:1]} | slice | bytes 1044480 | tf_op jit(solution)/shard_map/slice | solution.py:109
  359.7 20.6 %slice.374 = f32[255,512]{0,1:T(8,128)} slice(f32[512,512]{0,1:T(8,128)} %get-tuple-element.134), slice={[2:512:2], [0:512:1]} | slice | bytes 1044480 | tf_op jit(solution)/shard_map/slice | solution.py:109
  480.4 8.6 pad.124
  489.1 10.0 %pad.125 = f32[256,512]{0,1:T(8,128)S(1)} pad(f32[128,512]{0,1:T(8,128)} %add.350, f32[]{:T(128)} %constant.74.clone.1), padding=1_0_1x0_0_0 | pad | bytes 786436 | tf_op jit(solution)/shard_map/pad | solution.py:109
  500.7 19.6 %pad.127 = f32[512,512]{0,1:T(8,128)S(1)} pad(f32[256,512]{0,1:T(8,128)} %add.352, f32[]{:T(128)} %constant.74.clone.1), padding=1_0_1x0_0_0 | pad | bytes 1572868 | tf_op jit(solution)/shard_map/pad | solution.py:109
  522.2 11.1 %pad.142 = f32[256,512]{0,1:T(8,128)} pad(f32[128,512]{0,1:T(8,128)} %pad_maximum_fusion.12, f32[]{:T(128)} %constant.74.clone.1), padding=0_1_1x0_0_0 | pad | bytes 786436 | tf_op jit(solution)/shard_map/pad | solution.py:109
  533.3 11.2 %pad.143 = f32[256,512]{0,1:T(8,128)} pad(f32[128,512]{0,1:T(8,128)} %add.361, f32[]{:T(128)} %constant.74.clone.1), padding=1_0_1x0_0_0 | pad | bytes 786436 | tf_op jit(solution)/shard_map/pad | solution.py:109
  550.5 21.9 %pad.126 = f32[512,512]{0,1:T(8,128)} pad(f32[256,512]{0,1:T(8,128)} %pad_maximum_fusion, f32[]{:T(128)} %constant.74.clone.1), padding=0_1_1x0_0_0 | pad | bytes 1572868 | tf_op jit(solution)/shard_map/pad | solution.py:109
  573.7 26.5 %all-gather.1 = f32[8,1,512]{2,1,0:T(1,128)S(1)} all-gather(f32[1,1,512]{2,1,0:T(1,128)S(1)} %bitcast.110), channel_id=1, replica_groups=mesh['sp'=8,'tp'=4] {'sp'}, dimensions={0}, use_global_device_ids=true | all-gather | bytes 18432 | tf_op jit(solution)/shard_map/all_gather | solution.py:18
  600.2 21.8 %pad.145 = f32[512,512]{0,1:T(8,128)} pad(f32[256,512]{0,1:T(8,128)} %add.362, f32[]{:T(128)} %constant.74.clone.1), padding=1_0_1x0_0_0 | pad | bytes 1572868 | tf_op jit(solution)/shard_map/pad | solution.py:109
  624.0 21.9 %pad.144 = f32[512,512]{0,1:T(8,128)} pad(f32[256,512]{0,1:T(8,128)} %pad_maximum_fusion.1, f32[]{:T(128)} %constant.74.clone.1), padding=0_1_1x0_0_0 | pad | bytes 1572868 | tf_op jit(solution)/shard_map/pad | solution.py:109
  647.2 26.1 %all-gather = f32[8,1,512]{2,1,0:T(1,128)S(1)} all-gather(f32[1,1,512]{2,1,0:T(1,128)S(1)} %bitcast.111), channel_id=1, replica_groups=mesh['sp'=8,'tp'=4] {'sp'}, dimensions={0}, use_global_device_ids=true | all-gather | bytes 18432 | tf_op jit(solution)/shard_map/all_gather | solution.py:18
  681.9 39.5 %reduce-scatter.2.cloned.1.call-done = f32[128,2048]{1,0:T(8,128)} async-done(((f32[512,2048]{1,0:T(8,128)}), f32[128,2048]{1,0:T(8,128)}) %reduce-scatter.2.cloned.1.call-update) | async-done | bytes 1048592 | tf_op jit(solution)/shard_map/reduce_scatter | solution.py:116
  727.8 42.2 %all_to_all.25 = bf16[8,48,2048]{2,1,0:T(8,128)(2,1)} all-to-all(bf16[8,48,2048]{2,1,0:T(8,128)(2,1)S(1)} %broadcast_select_fusion), channel_id=1, replica_groups=mesh['sp'=8,'tp'=4] {'sp'}, dimensions={0} | all-to-all | bytes 3145728 | tf_op jit(solution)/shard_map/all_to_all | solution.py:139
  770.1 44.5 %all-gather.5.cloned.1.call-done = bf16[4,384,2048]{2,1,0:T(8,128)(2,1)} async-done(((bf16[1,384,2048]{2,1,0:T(8,128)(2,1)}), bf16[4,384,2048]{2,1,0:T(8,128)(2,1)}) %all-gather.5.cloned.1.call-update) | async-done | bytes 6291472 | tf_op jit(solution)/shard_map/all_gather | solution.py:140
  825.8 46.5 %all-gather.7.cloned.1.call-done = bf16[1536,2048]{1,0:T(8,128)(2,1)} async-done(((bf16[1536,512]{1,0:T(8,128)(2,1)}), bf16[1536,2048]{1,0:T(8,128)(2,1)}) %all-gather.7.cloned.1.call-update) | async-done | bytes 6291472 | tf_op jit(solution)/shard_map/all_gather | solution.py:58
  879.2 22.7 %all_to_all.26 = bf16[4,384,512]{2,1,0:T(8,128)(2,1)S(1)} all-to-all(bf16[4,384,512]{2,1,0:T(8,128)(2,1)S(1)} %bitcast.94), channel_id=1, replica_groups=mesh['sp'=8,'tp'=4] {'tp'}, dimensions={0} | all-to-all | bytes 3145728 | tf_op jit(solution)/shard_map/all_to_all | solution.py:148
  914.1 36.2 %all-to-all-done.2 = bf16[8,48,2048]{2,1,0:T(8,128)(2,1)S(1)} async-done(((bf16[8,48,2048]{2,1,0:T(8,128)(2,1)}), bf16[8,48,2048]{2,1,0:T(8,128)(2,1)S(1)}, u32[]{:S(2)}, u32[]{:S(2)}) %all-to-all-start.2) | async-done | bytes 1572896 | tf_op jit(solution)/shard_map/all_to_all | solution.py:155
  (264 shorter events, 315.8 us)
Async XLA Ops:
  6.5 667.2 %copy-start = (bf16[512,2048]{1,0:T(8,128)(2,1)S(1)}, bf16[512,2048]{1,0:T(8,128)(2,1)}, u32[]{:S(2)}) copy-start(bf16[512,2048]{1,0:T(8,128)(2,1)} %param.25) | copy-start | bytes 6291460
  6.5 11.3 %copy-start.25 = (bf16[512,512]{1,0:T(8,128)(2,1)S(1)}, bf16[512,512]{1,0:T(8,128)(2,1)}, u32[]{:S(2)}) copy-start(bf16[512,512]{1,0:T(8,128)(2,1)} %param.19) | copy-start | bytes 1572868
  6.5 714.9 %reduce-scatter.2.cloned.1.call-start = ((), (), s32[]{:S(2)}) async-start(), calls=%async_computation.4 | async-start | bytes 5242880 | tf_op jit(solution)/shard_map/reduce_scatter | solution.py:116
  7.6 11.3 %collective-permute-start = (bf16[3,512]{0,1:T(8,128)(2,1)S(1)}, bf16[3,512]{0,1:T(8,128)(2,1)S(1)}, u32[]{:S(2)}, u32[]{:S(2)}) collective-permute-start(bf16[3,512]{0,1:T(8,128)(2,1)S(1)} %copy.90), channel_id=1, source_target_pairs={{0,4},{4,8},{8,12},{12,16},{16,20},{20,24},{24,28},{1,5},{5,9},{9,... | collective-permute-start | bytes 9224 | tf_op jit(solution)/shard_map/ppermute | solution.py:13
  19.2 1.3 copy-start.30
  265.9 1.5 copy-start.11
  265.9 1.5 copy-start.12
  388.7 4.2 copy-start.16
  388.7 6.9 copy-start.8
  393.7 8.5 copy-start.10
  402.3 6.6 copy-start.7
  407.0 6.4 copy-start.9
  414.2 3.7 copy-start.18
  414.2 7.4 copy-start.6
  419.6 8.9 copy-start.5
  430.2 6.6 copy-start.4
  434.9 7.5 copy-start.3
  447.3 8.9 copy-start.2
  477.0 3.3 copy-start.23
  489.0 10.1 %copy-start.13 = (f32[256,512]{0,1:T(8,128)}, f32[256,512]{0,1:T(8,128)S(1)}, u32[]{:S(2)}) copy-start(f32[256,512]{0,1:T(8,128)S(1)} %pad.124) | copy-start | bytes 1572868
  489.0 31.3 %copy-start.22 = (f32[1,512]{0,1:T(8,128)S(1)}, f32[1,512]{0,1:T(8,128)}, u32[]{:S(2)}) copy-start(f32[1,512]{0,1:T(8,128)} %slice.434) | copy-start | bytes 6148
  546.6 2.9 copy-start.21
  550.5 71.4 %copy-start.20 = (f32[1,512]{0,1:T(8,128)S(1)}, f32[1,512]{0,1:T(8,128)}, u32[]{:S(2)}) copy-start(f32[1,512]{0,1:T(8,128)} %slice.433) | copy-start | bytes 6148
  679.3 42.1 %copy-start.24 = (bf16[128,2048]{1,0:T(8,128)(2,1)S(1)}, bf16[128,2048]{1,0:T(8,128)(2,1)}, u32[]{:S(2)}) copy-start(bf16[128,2048]{1,0:T(8,128)(2,1)} %param.17) | copy-start | bytes 1572868
  679.3 43.6 %copy-start.26 = (f32[2048]{0:T(1024)S(1)}, f32[2048]{0:T(1024)}, u32[]{:S(2)}) copy-start(f32[2048]{0:T(1024)} %param.26) | copy-start | bytes 24580
  679.4 135.3 %all-gather.5.cloned.1.call-start = ((), (), s32[]{:S(2)}) async-start(), calls=%async_computation.5 | async-start | bytes 7864320 | tf_op jit(solution)/shard_map/all_gather | solution.py:140
  770.1 102.2 %all-gather.7.cloned.1.call-start = ((), (), s32[]{:S(2)}) async-start(), calls=%async_computation.6 | async-start | bytes 7864320 | tf_op jit(solution)/shard_map/all_gather | solution.py:58
  814.7 6.3 copy-start.28
  814.7 6.3 copy-start.29
  908.1 5.9 copy-start.27
  908.1 42.3 %all-to-all-start.2 = ((bf16[8,48,2048]{2,1,0:T(8,128)(2,1)}), bf16[8,48,2048]{2,1,0:T(8,128)(2,1)S(1)}, u32[]{:S(2)}, u32[]{:S(2)}) async-start(bf16[8,48,2048]{2,1,0:T(8,128)(2,1)} %reshape.145), calls=%async_computation.3 | async-start | bytes 3145728 | tf_op jit(solution)/shard_map/all_to_all | solution.py:155
  952.7 9.2 copy-start.1
  (5 other events, 4.6 us)
Sparse Core Ops, SparseCore 0:
  679.5 41.9 reduce-scatter.1
  770.2 44.4 all-gather.4
  826.0 46.3 all-gather.6
where the time goes:
time: 977 us; the launch traced here: 969 us
  local copies, waits for them, and re-layouts  555 us (57%)
  waiting for transfers between devices  167 us (17%)
  blocking collectives  118 us (12%)
  other arithmetic  80.4 us (8%)
  matrix products  24.5 us (3%)
  between operations  14 us (1%)
  starting transfers between devices  10.6 us (1%)
    slice x50, local copies, waits for them, and re-layouts, body(): lax.associative_scan(chain_step, (decay, drive), axis=0)  338 us
    pad x32, local copies, waits for them, and re-layouts, body(): lax.associative_scan(chain_step, (decay, drive), axis=0)  183 us
    all_gather x2, blocking collectives, entering(): everything = jax.tree.map(lambda part: lax.all_gather(part, axis), x)  52.6 us
    all_gather x1, waiting for transfers between devices, expert_down(): lax.all_gather(active, 'tp', axis=1, tiled=True)  46.5 us
    all_gather x1, waiting for transfers between devices, body(): lax.all_gather(arrived.reshape(1, experts * capacity, model_width), 'tp',...  44.5 us
    all_to_all x1, blocking collectives, body(): lax.all_to_all(outgoing, 'sp', split_axis=0, concat_axis=0, tiled=True)  42.2 us
    reduce_scatter x1, waiting for transfers between devices, body(): lax.psum_scatter(jnp.dot(branch, output_projection_weight, preferred_elem...  39.5 us
    all_to_all x1, waiting for transfers between devices, body(): lax.all_to_all(joined.reshape(experts, capacity, model_width), 'sp', spli...  36.2 us
  transfers between devices with their start and end apart: 5, of which 4 were waited for; matrix products, arithmetic and copies ran while one was open for 1% of the time, Pallas kernels for 0%

commit v1 on v0

--- a/solution.py
+++ b/solution.py
@@ -1,6 +1,8 @@
 import jax
 import jax.numpy as jnp
 from jax import lax
+from jax.experimental import pallas as pl
+from jax.experimental.pallas import tpu as pltpu
 from jax.sharding import PartitionSpec as P
 
 RECURRENT_SCALE = 8.0
@@ -13,23 +15,134 @@
     return lax.ppermute(block, axis, route)
 
 
-def entering(x, axis, combine, identity):
-    size, position = (lax.axis_size(axis), lax.axis_index(axis))
-    everything = jax.tree.map(lambda part: lax.all_gather(part, axis), x)
-    start = jax.tree.map(
-        lambda part, zero: jnp.broadcast_to(jnp.asarray(zero, part.dtype), part.shape), x, identity
-    )
-
-    def lap(k, before):
-        reached = k < position
-        new = combine(before, jax.tree.map(lambda part: part[k], everything))
-        return jax.tree.map(lambda a, b: jnp.where(reached, a, b), new, before)
-
-    return lax.fori_loop(0, size, lap, start)
-
-
-def chain_step(earlier, later):
-    return (earlier[0] * later[0], later[0] * earlier[1] + later[1])
+LANES = 128
+SEGMENTS = 8
+
+
+def block_diagonal(blocks):
+    count, width, _ = blocks.shape
+    empty = jnp.zeros((width, width), blocks.dtype)
+    rows = []
+    for i in range(count):
+        rows.append(jnp.concatenate([blocks[i] if j == i else empty for j in range(count)], axis=1))
+    return jnp.concatenate(rows, axis=0)
+
+
+def scan_kernel(rim, x, taps, recur, inward, slope, boost, local, running, total, wide, decays, drives):
+    tokens, lanes = x.shape
+    margin = rim.shape[0]
+    count = taps.shape[0]
+    wide[0:margin, :] = rim[...].astype(jnp.float32)
+    wide[margin : margin + tokens, :] = x[...].astype(jnp.float32)
+    first = margin - count + 1
+    mixed = wide[first : first + tokens, :] * taps[0:1, :]
+    for j in range(1, count):
+        mixed = mixed + wide[first + j : first + j + tokens, :] * taps[j : j + 1, :]
+    smoothed = mixed.astype(jnp.bfloat16)
+    recur_gate = jax.nn.sigmoid(
+        jnp.dot(smoothed, block_diagonal(recur), preferred_element_type=jnp.float32)
+    )
+    input_gate = jax.nn.sigmoid(
+        jnp.dot(smoothed, block_diagonal(inward), preferred_element_type=jnp.float32)
+    )
+    log_decay = -RECURRENT_SCALE * recur_gate * slope[...] + boost[...]
+    decay = jnp.exp(log_decay)
+    twice = 2.0 * log_decay
+    series = 1.0 + twice * (1.0 / 9.0)
+    for n in range(8, 1, -1):
+        series = 1.0 + twice * (1.0 / n) * series
+    lost = jnp.where(twice > -0.35, -twice * series, 1.0 - decay * decay)
+    decays[...] = decay
+    drives[...] = jnp.sqrt(lost) * (input_gate * smoothed.astype(jnp.float32))
+    length = tokens // SEGMENTS
+
+    def step(j, held):
+        product, state = held
+        here = pl.ds(j, SEGMENTS, stride=length)
+        a = decays[here, :]
+        state = a * state + drives[here, :]
+        product = product * a
+        local[here, :] = state
+        running[here, :] = product
+        return product, state
+
+    product, state = lax.fori_loop(
+        0,
+        length,
+        step,
+        (jnp.ones((SEGMENTS, lanes), jnp.float32), jnp.zeros((SEGMENTS, lanes), jnp.float32)),
+        unroll=8,
+    )
+    a, b = product[0:1], state[0:1]
+    for k in range(1, SEGMENTS):
+        a, b = a * product[k : k + 1], product[k : k + 1] * b + state[k : k + 1]
+    total[0:1, :] = a
+    total[1:2, :] = b
+
+
+def local_scan(rim, x, taps, recur, inward, slope, boost):
+    tokens, channels = x.shape
+    lanes = min(LANES, channels)
+    width = recur.shape[1]
+    column = lambda rows: pl.BlockSpec((rows, lanes), lambda i: (0, i))
+    blocks = pl.BlockSpec((lanes // width, width, width), lambda i: (i, 0, 0))
+    wide = jax.ShapeDtypeStruct((tokens, channels), jnp.float32)
+    return pl.pallas_call(
+        scan_kernel,
+        grid=(channels // lanes,),
+        in_specs=[
+            column(rim.shape[0]),
+            column(tokens),
+            column(taps.shape[0]),
+            blocks,
+            blocks,
+            column(1),
+            column(tokens),
+        ],
+        out_specs=[column(tokens), column(tokens), column(2)],
+        out_shape=[wide, wide, jax.ShapeDtypeStruct((2, channels), jnp.float32)],
+        scratch_shapes=[
+            pltpu.VMEM((tokens + rim.shape[0], lanes), jnp.float32),
+            pltpu.VMEM((tokens, lanes), jnp.float32),
+            pltpu.VMEM((tokens, lanes), jnp.float32),
+        ],
+        name="local_scan",
+    )(rim, x, taps, recur, inward, slope, boost)
+
+
+def branch_kernel(position, totals, local, running, gate, branch):
+    tokens, lanes = local.shape
+    entering = jnp.zeros((1, lanes), jnp.float32)
+    for k in range(totals.shape[0]):
+        passed = totals[k, 0:1, :] * entering + totals[k, 1:2, :]
+        entering = jnp.where(k < position[0], passed, entering)
+    length = tokens // SEGMENTS
+    for k in range(SEGMENTS):
+        here = slice(k * length, (k + 1) * length)
+        state = local[here, :] + running[here, :] * entering
+        opened = jax.nn.gelu(gate[here, :].astype(jnp.float32))
+        branch[here, :] = (opened * state).astype(jnp.bfloat16)
+        entering = state[length - 1 : length]
+
+
+def finish_branch(position, totals, local, running, gate):
+    tokens, channels = local.shape
+    lanes = min(LANES, channels)
+    column = lambda rows: pl.BlockSpec((rows, lanes), lambda i: (0, i))
+    return pl.pallas_call(
+        branch_kernel,
+        grid=(channels // lanes,),
+        in_specs=[
+            pl.BlockSpec(memory_space=pltpu.SMEM),
+            pl.BlockSpec((totals.shape[0], 2, lanes), lambda i: (0, 0, i)),
+            column(tokens),
+            column(tokens),
+            column(tokens),
+        ],
+        out_specs=column(tokens),
+        out_shape=jax.ShapeDtypeStruct((tokens, channels), jnp.bfloat16),
+        name="finish_branch",
+    )(position, totals, local, running, gate)
 
 
 def slot_numbers(picks, experts):
@@ -79,38 +192,20 @@
     down_weight,
 ):
     tokens_here, channels = recurrent_input.shape
-    taps = filter_weight.shape[0]
-    rim = shifted(recurrent_input[tokens_here - taps + 1 :], "sp", 1)
-    extended = jnp.concatenate([rim, recurrent_input], axis=0).astype(jnp.float32)
-    mixed_in = extended[0:tokens_here] * filter_weight[0]
-    for offset in range(1, taps):
-        mixed_in = mixed_in + extended[offset : offset + tokens_here] * filter_weight[offset]
-    smoothed = mixed_in.astype(jnp.bfloat16)
-    grouped = smoothed.reshape(
-        tokens_here, recurrence_gate_matrix.shape[0], recurrence_gate_matrix.shape[1]
-    )
-    recurrence_gate = jax.nn.sigmoid(
-        jnp.einsum(
-            "tni,nij->tnj", grouped, recurrence_gate_matrix, preferred_element_type=jnp.float32
-        ).reshape(tokens_here, channels)
-    )
-    input_gate = jax.nn.sigmoid(
-        jnp.einsum(
-            "tni,nij->tnj", grouped, input_gate_matrix, preferred_element_type=jnp.float32
-        ).reshape(tokens_here, channels)
-    )
-    decay_logarithm = (
-        -RECURRENT_SCALE * recurrence_gate * jax.nn.softplus(-channel_decay_raw) + token_decay_boost
-    )
-    decay = jnp.exp(decay_logarithm)
-    drive = jnp.sqrt(-jnp.expm1(2.0 * decay_logarithm)) * (
-        input_gate * smoothed.astype(jnp.float32)
-    )
-    running, local_state = lax.associative_scan(chain_step, (decay, drive), axis=0)
-    identity = (jnp.ones((channels,), jnp.float32), jnp.zeros((channels,), jnp.float32))
-    carried = entering((running[-1], local_state[-1]), "sp", chain_step, identity)
-    state = local_state + running * carried[1][None, :]
-    branch = (jax.nn.gelu(recurrent_out_gate.astype(jnp.float32)) * state).astype(jnp.bfloat16)
+    rim = shifted(recurrent_input[tokens_here - 8 :], "sp", 1)
+    slope = jax.nn.softplus(-channel_decay_raw)[None, :]
+    local, running, total = local_scan(
+        rim,
+        recurrent_input,
+        filter_weight,
+        recurrence_gate_matrix,
+        input_gate_matrix,
+        slope,
+        token_decay_boost,
+    )
+    totals = lax.all_gather(total, "sp")
+    position = lax.axis_index("sp").astype(jnp.int32).reshape(1)
+    branch = finish_branch(position, totals, local, running, recurrent_out_gate)
     tp_size = lax.axis_size("tp")
     rows_dev = tokens_here // tp_size
     projected = lax.psum_scatter(

time: 977 us -> 359 us (0.37)
  local copies, waits for them, and re-layouts: 555 us -> 20.2 us
  other arithmetic: 80.4 us -> 12.2 us
  blocking collectives: 118 us -> 99.2 us
  Pallas kernels: 0 us -> 11.4 us
    slice x54 -> x2, local copies, waits for them, and re-layouts: 340 us -> 1.06 us  [the longest x1 0.85 us: body(): rim = shifted(recurrent_input[tokens_here - 8:], 'sp', 1)]
    pad x32 -> x0, local copies, waits for them, and re-layouts: 183 us -> none  [body(): lax.associative_scan(chain_step, (decay, drive), axis=0)]
    add x32 -> x0, other arithmetic: 44.7 us -> none  [the longest x17 27 us: chain_step(): return (earlier[0] * later[0], later[0] * earlier[1] + later[1])]
    all_gather x2 -> x1, blocking collectives: 52.6 us -> 34.5 us  [body(): totals = lax.all_gather(total, 'sp')]
    concatenate x16 -> x0, other arithmetic: 11.6 us -> none  [body(): lax.associative_scan(chain_step, (decay, drive), axis=0)]
    pallas_call x0 -> x2, Pallas kernels: none -> 11.4 us  [the longest x1 7.62 us: local_scan(): pl.pallas_call(scan_kernel, grid=(channels // lanes,), in_specs=[column(r...]
    unnamed x76 -> x13, local copies, waits for them, and re-layouts: 11.5 us -> 0.73 us
  transfers between devices with their start and end apart: 5 -> 5, of which waited for: 4 -> 5; matrix products, arithmetic and copies ran while one was open for 1% -> 1% of each run, Pallas kernels for 0% -> 0%
where the time goes in v1:
time: 359 us; the launch traced here: 358 us
  waiting for transfers between devices  169 us (47%)
  blocking collectives  99.2 us (28%)
  matrix products  22.1 us (6%)
  local copies, waits for them, and re-layouts  20.2 us (6%)
  between operations  13.3 us (4%)
  other arithmetic  12.2 us (3%)
  Pallas kernels  11.4 us (3%)
  starting transfers between devices  10.6 us (3%)
    all_gather x1, waiting for transfers between devices, expert_down(): lax.all_gather(active, 'tp', axis=1, tiled=True)  46.5 us
    all_gather x1, waiting for transfers between devices, body(): lax.all_gather(arrived.reshape(1, experts * capacity, model_width), 'tp',...  44.5 us
    all_to_all x1, blocking collectives, body(): lax.all_to_all(outgoing, 'sp', split_axis=0, concat_axis=0, tiled=True)  42.3 us
    reduce_scatter x1, waiting for transfers between devices, body(): lax.psum_scatter(jnp.dot(branch, output_projection_weight, preferred_elem...  41.8 us
    all_to_all x1, waiting for transfers between devices, body(): lax.all_to_all(joined.reshape(experts, capacity, model_width), 'sp', spli...  36.3 us
    all_gather x1, blocking collectives, body(): totals = lax.all_gather(total, 'sp')  34.5 us
    all_to_all x1, blocking collectives, body(): lax.all_to_all(result.reshape(tp_size, experts * capacity, -1), 'tp', spl...  22.5 us
    pallas_call x1, Pallas kernels, local_scan(): pl.pallas_call(scan_kernel, grid=(channels // lanes,), in_specs=[column(r...  7.62 us
  transfers between devices with their start and end apart: 5, of which 5 were waited for; matrix products, arithmetic and copies ran while one was open for 1% of the time, Pallas kernels for 0%

profile of v1, /device:TPU:0, one launch (start us, length us, event | category | flops | bytes accessed | tf_op | source)
XLA Modules:
  0.0 358.3 jit_solution(3788383922061402294)
XLA Ops:
  6.5 0.8 slice.9
  7.4 4.9 %collective-permute-start = (bf16[8,512]{1,0:T(8,128)(2,1)S(1)}, bf16[8,512]{1,0:T(8,128)(2,1)S(1)}, u32[]{:S(2)}, u32[]{:S(2)}) collective-permute-start(bf16[8,512]{1,0:T(8,128)(2,1)S(1)} %slice.9), channel_id=1, source_target_pairs={{0,4},{4,8},{8,12},{12,16},{16,20},{20,24},{24,28},{1,5},{5,9},{9,... | collective-permute-start | bytes 24584 | tf_op jit(solution)/shard_map/ppermute | solution.py:15
  12.3 1.3 compare_select_fusion.2
  13.6 0.6 copy-done.2
  14.2 7.6 %local_scan.1 = (f32[512,512]{1,0:T(8,128)}, f32[512,512]{1,0:T(8,128)}, f32[2,512]{1,0:T(2,128)}) custom-call(bf16[8,512]{1,0:T(8,128)(2,1)} %copy-done.2, bf16[512,512]{1,0:T(8,128)(2,1)} %x.1, f32[4,512]{1,0:T(4,128)} %taps.1, bf16[8,64,64]{2,1,0:T(8,128)(2,1)} %recur.1, bf16[8,64,64]{2,1,0:T(8,128)(2,1)} %inward.1, f32[1,512]{1,0:T(1,128)} %bitcast.40, ...), custom_call_target="tpu_custom_call" | custom-call | tf_op jit(solution)/shard_map/local_scan/pallas_call | solution.py:90
  21.8 34.5 %all-gather.1.totals = f32[8,2,512]{2,1,0:T(2,128)} all-gather(f32[1,2,512]{2,1,0:T(2,128)} %bitcast.41), channel_id=2, replica_groups=mesh['sp'=8,'tp'=4] {'sp'}, dimensions={0}, use_global_device_ids=true | all-gather | bytes 36864 | tf_op jit(solution)/shard_map/all_gather | solution.py:206
  56.3 3.8 %finish_branch.1 = bf16[512,512]{1,0:T(8,128)(2,1)} custom-call(s32[1]{0:T(128)} %bitcast.position, f32[8,2,512]{2,1,0:T(2,128)} %all-gather.1.totals, f32[512,512]{1,0:T(8,128)} %get-tuple-element.9.local, f32[512,512]{1,0:T(8,128)} %get-tuple-element.10.running, bf16[512,512]{1,0:T(8,128)(2,1)} %gate.1), custom_call_target="tpu_custom_call" | custom-call | tf_op jit(solution)/shard_map/finish_branch/pallas_call | solution.py:132
  60.1 4.2 %fusion.14 = f32[512,2048]{1,0:T(8,128)} fusion(bf16[512,512]{1,0:T(8,128)(2,1)} %finish_branch.1, bf16[512,2048]{1,0:T(8,128)(2,1)S(1)} %copy-done), kind=kOutput, calls=%fused_computation.43 | convolution fusion | flops 1073741824 | bytes 6815744 | tf_op jit(solution)/shard_map/dot_general | solution.py:212
  64.4 0.7 broadcast_multiply_fusion
  65.5 0.6 reduce-window.6
  66.1 0.2 slice_reduce_fusion
  66.7 0.2 select_reduce_fusion
  66.9 41.8 %reduce-scatter.2.cloned.1.call-done = f32[128,2048]{1,0:T(8,128)} async-done(((f32[512,2048]{1,0:T(8,128)}), f32[128,2048]{1,0:T(8,128)}) %reduce-scatter.2.cloned.1.call-update) | async-done | bytes 1048592 | tf_op jit(solution)/shard_map/reduce_scatter | solution.py:211
  108.7 1.6 fusion.5
  110.3 0.2 fusion.7
  110.5 3.1 gather_fusion
  113.6 1.6 broadcast_select_fusion
  115.2 42.3 %all_to_all.25 = bf16[8,48,2048]{2,1,0:T(8,128)(2,1)} all-to-all(bf16[8,48,2048]{2,1,0:T(8,128)(2,1)S(1)} %broadcast_select_fusion), channel_id=1, replica_groups=mesh['sp'=8,'tp'=4] {'sp'}, dimensions={0} | all-to-all | bytes 3145728 | tf_op jit(solution)/shard_map/all_to_all | solution.py:234
  157.5 44.5 %all-gather.5.cloned.1.call-done = bf16[4,384,2048]{2,1,0:T(8,128)(2,1)} async-done(((bf16[1,384,2048]{2,1,0:T(8,128)(2,1)}), bf16[4,384,2048]{2,1,0:T(8,128)(2,1)}) %all-gather.5.cloned.1.call-update) | async-done | bytes 6291472 | tf_op jit(solution)/shard_map/all_gather | solution.py:235
  202.1 6.3 %fusion.3 = f32[1536,512]{1,0:T(8,128)S(1)} fusion(bf16[1536,2048]{1,0:T(8,128)(2,1)} %bitcast.43, bf16[1,2048,512]{2,1,0:T(8,128)(2,1)} %param.27), kind=kOutput, calls=%fused_computation.7 | convolution fusion | flops 3221225472 | bytes 11534336 | tf_op jit(solution)/shard_map/dot_general | solution.py:163
  208.4 4.8 %fusion = bf16[1536,512]{1,0:T(8,128)(2,1)} fusion(bf16[1536,2048]{1,0:T(8,128)(2,1)S(1)} %bitcast.44, f32[1536,512]{1,0:T(8,128)S(1)} %fusion.3, bf16[1,2048,512]{2,1,0:T(8,128)(2,1)S(1)} %copy-done.5), kind=kOutput, calls=%fused_computation.3 | convolution fusion | flops 3225944064 | bytes 13107200 | tf_op jit(solution)/shard_map/dot_general | solution.py:164
  213.2 46.5 %all-gather.7.cloned.1.call-done = bf16[1536,2048]{1,0:T(8,128)(2,1)} async-done(((bf16[1536,512]{1,0:T(8,128)(2,1)}), bf16[1536,2048]{1,0:T(8,128)(2,1)}) %all-gather.7.cloned.1.call-update) | async-done | bytes 6291472 | tf_op jit(solution)/shard_map/all_gather | solution.py:171
  259.7 6.8 %convolution_convert_fusion = bf16[1536,512]{1,0:T(8,128)(2,1)S(1)} fusion(bf16[1536,2048]{1,0:T(8,128)(2,1)} %all-gather.7.cloned.1.call-done, bf16[1,2048,512]{2,1,0:T(8,128)(2,1)} %param.29), kind=kOutput, calls=%fused_computation.4 | convolution fusion | flops 3222011904 | bytes 9961472 | tf_op jit(solution)/shard_map/dot_general | solution.py:170
  266.6 22.5 %all_to_all.26 = bf16[4,384,512]{2,1,0:T(8,128)(2,1)S(1)} all-to-all(bf16[4,384,512]{2,1,0:T(8,128)(2,1)S(1)} %bitcast.38), channel_id=1, replica_groups=mesh['sp'=8,'tp'=4] {'tp'}, dimensions={0} | all-to-all | bytes 3145728 | tf_op jit(solution)/shard_map/all_to_all | solution.py:243
  289.1 2.4 copy.29
  291.4 3.8 %reshape.129 = bf16[8,48,2048]{2,1,0:T(8,128)(2,1)} reshape(bf16[1,384,4,512]{3,2,1,0:T(4,128)(2,1)} %copy.29) | data formatting | bytes 3145728 | tf_op jit(solution)/shard_map/reshape | solution.py:251
  295.3 5.6 %all-to-all-start.2 = ((bf16[8,48,2048]{2,1,0:T(8,128)(2,1)}), bf16[8,48,2048]{2,1,0:T(8,128)(2,1)}, u32[]{:S(2)}, u32[]{:S(2)}) async-start(bf16[8,48,2048]{2,1,0:T(8,128)(2,1)} %reshape.129), calls=%async_computation.3 | async-start | bytes 3145728 | tf_op jit(solution)/shard_map/all_to_all | solution.py:250
  301.3 36.3 %all-to-all-done.2 = bf16[8,48,2048]{2,1,0:T(8,128)(2,1)} async-done(((bf16[8,48,2048]{2,1,0:T(8,128)(2,1)}), bf16[8,48,2048]{2,1,0:T(8,128)(2,1)}, u32[]{:S(2)}, u32[]{:S(2)}) %all-to-all-start.2) | async-done | bytes 1572896 | tf_op jit(solution)/shard_map/all_to_all | solution.py:250
  337.6 5.0 %gather_fusion.1 = bf16[256,2048]{1,0:T(8,128)(2,1)} fusion(bf16[384,2048]{1,0:T(8,128)(2,1)} %bitcast.14, s32[1024]{0:T(1024)S(1)} %pad_clamp_fusion), kind=kCustom, calls=%fused_computation.1 | custom fusion | bytes 2098176 | tf_op jit(solution)/shard_map/gather | solution.py:258
  342.6 3.4 reshape.131
  346.0 4.8 %multiply_reduce_fusion = f32[128,2048]{1,0:T(8,128)S(1)} fusion(f32[128,2,2048]{2,1,0:T(2,128)} %reshape.131, f32[128,2]{1,0:T(8,128)S(1)} %copy.31), kind=kLoop, calls=%fused_computation.9 | loop fusion | flops 786432 | bytes 3146752 | tf_op jit(solution)/shard_map/reduce_sum | solution.py:262
  350.8 0.9 fusion.8
  (36 shorter events, 1.4 us)
Async XLA Ops:
  6.5 53.6 %copy-start = (bf16[512,2048]{1,0:T(8,128)(2,1)S(1)}, bf16[512,2048]{1,0:T(8,128)(2,1)}, u32[]{:S(2)}) copy-start(bf16[512,2048]{1,0:T(8,128)(2,1)} %param.23) | copy-start | bytes 6291460
  6.5 102.1 %reduce-scatter.2.cloned.1.call-start = ((), (), s32[]{:S(2)}) async-start(), calls=%async_computation.4 | async-start | bytes 5242880 | tf_op jit(solution)/shard_map/reduce_scatter | solution.py:211
  7.4 6.2 %collective-permute-start = (bf16[8,512]{1,0:T(8,128)(2,1)S(1)}, bf16[8,512]{1,0:T(8,128)(2,1)S(1)}, u32[]{:S(2)}, u32[]{:S(2)}) collective-permute-start(bf16[8,512]{1,0:T(8,128)(2,1)S(1)} %slice.9), channel_id=1, source_target_pairs={{0,4},{4,8},{8,12},{12,16},{16,20},{20,24},{24,28},{1,5},{5,9},{9,... | collective-permute-start | bytes 24584 | tf_op jit(solution)/shard_map/ppermute | solution.py:15
  13.6 0.6 copy-start.2
  64.3 45.9 %copy-start.1 = (f32[2048]{0:T(1024)S(1)}, f32[2048]{0:T(1024)}, u32[]{:S(2)}) copy-start(f32[2048]{0:T(1024)} %param.24) | copy-start | bytes 24580
  64.4 137.7 %all-gather.5.cloned.1.call-start = ((), (), s32[]{:S(2)}) async-start(), calls=%async_computation.5 | async-start | bytes 7864320 | tf_op jit(solution)/shard_map/all_gather | solution.py:235
  157.5 102.2 %all-gather.7.cloned.1.call-start = ((), (), s32[]{:S(2)}) async-start(), calls=%async_computation.6 | async-start | bytes 7864320 | tf_op jit(solution)/shard_map/all_gather | solution.py:171
  202.1 6.3 %copy-start.4 = (bf16[4,384,2048]{2,1,0:T(8,128)(2,1)S(1)}, bf16[4,384,2048]{2,1,0:T(8,128)(2,1)}, u32[]{:S(2)}) copy-start(bf16[4,384,2048]{2,1,0:T(8,128)(2,1)} %all-gather.5.cloned.1.call-done) | copy-start | bytes 18874372
  202.1 6.3 %copy-start.5 = (bf16[1,2048,512]{2,1,0:T(8,128)(2,1)S(1)}, bf16[1,2048,512]{2,1,0:T(8,128)(2,1)}, u32[]{:S(2)}) copy-start(bf16[1,2048,512]{2,1,0:T(8,128)(2,1)} %param.28) | copy-start | bytes 6291460
  295.3 5.9 %copy-start.3 = (f32[128,2]{0,1:T(2,128)S(1)}, f32[128,2]{0,1:T(2,128)}, u32[]{:S(2)}) copy-start(f32[128,2]{0,1:T(2,128)} %param.26) | copy-start | bytes 3076
  295.3 42.4 %all-to-all-start.2 = ((bf16[8,48,2048]{2,1,0:T(8,128)(2,1)}), bf16[8,48,2048]{2,1,0:T(8,128)(2,1)}, u32[]{:S(2)}, u32[]{:S(2)}) async-start(bf16[8,48,2048]{2,1,0:T(8,128)(2,1)} %reshape.129), calls=%async_computation.3 | async-start | bytes 3145728 | tf_op jit(solution)/shard_map/all_to_all | solution.py:250
Sparse Core Ops, SparseCore 0:
  64.5 44.1 reduce-scatter.1
  157.6 44.4 all-gather.4
  213.3 46.3 all-gather.6
